TPU v7x, 32 devices: a whole 2x2x4 slice. The times are simulated.
32 devices in a mesh: sp: 4 (over z), tp: 8 (over y, x, core).
Axes of the slice: x: 2, y: 2, z: 4, core: 2. Of those that a mesh axis runs over, the one named last changes fastest.
Arguments:
- activations: bfloat16 [1024, 2048], P('sp', 'tp'), may hold values from -170 to 170
- norm_gain: float32 [2048], replicated, may hold values from 0.1 to 1.9
- query_weight: bfloat16 [2048, 1536], P(None, 'tp'), may hold values from -0.125 to 0.125
- latent_weight: bfloat16 [2048, 512], P(None, 'tp'), may hold values from -0.125 to 0.125
- rope_key_weight: bfloat16 [2048, 64], replicated, may hold values from -0.125 to 0.125
- latent_gain: float32 [512], replicated, may hold values from 1.5 to 64
- expand_weight: bfloat16 [512, 2048], P(None, 'tp'), may hold values from -0.25 to 0.25
- gate_weight: bfloat16 [2048, 1024], P(None, 'tp'), may hold values from -0.125 to 0.125
- pre_weight: bfloat16 [2048, 1024], P(None, 'tp'), may hold values from -0.125 to 0.125
- value_weight: bfloat16 [2048, 1024], P(None, 'tp'), may hold values from -0.125 to 0.125
- conv_kernel: bfloat16 [3, 1024], P(None, 'tp'), may hold values from -3.5 to 3.5
- output_attend: bfloat16 [1024, 2048], P('tp'), may hold values from -0.1875 to 0.1875
- output_conv: bfloat16 [1024, 2048], P('tp'), may hold values from -0.125 to 0.125
Outputs:
- mixed: bfloat16 [1024, 2048], P(('sp', 'tp'))
- log_weight_sum: float32 [8, 1024], P('tp', 'sp')
All inputs are finite; a program needn't handle non-finite values.
Results may differ from a plain program's by a relative error of at most 0.035.
The roundings to bfloat16 on the way count: a program that leaves them out, or rounds other values in their place, can miss the bound.
Values may be sent and summed in bfloat16 or wider, within the bound.
A program may use at most 128 MiB of HBM per device.

v0:
```python
import math
import jax
import jax.numpy as jnp
from jax import lax
from jax.sharding import PartitionSpec as P

D = 2048
NOPE = 128
ROPE = 64
VDIM = 128
GRID_W = 64
EPSILON = 1e-06
ROPE_BASE = 10000.0


def with_halo(array, sides, width):
    for axis, dim in sides:
        peers, length = (lax.axis_size(axis), array.shape[dim])
        up = [(i, (i + 1) % peers) for i in range(peers - 1)]
        down = [(j, i) for i, j in up]
        last = lax.slice_in_dim(array, length - width, length, axis=dim)
        leading = lax.slice_in_dim(array, 0, width, axis=dim)
        before = lax.ppermute(last, axis, up)
        after = lax.ppermute(leading, axis, down)
        array = jnp.concatenate([before, array, after], axis=dim)
    return array


def rotate(inputs, grid_rows, grid_cols):
    quarter = inputs.shape[-1] // 4
    inverse = ROPE_BASE ** (-jnp.arange(quarter, dtype=jnp.float32) / quarter)
    row_angle = (grid_rows[:, None] * inverse)[:, None, :]
    col_angle = (grid_cols[:, None] * inverse)[:, None, :]
    part_one = inputs[..., :quarter]
    part_two = inputs[..., quarter : 2 * quarter]
    part_three = inputs[..., 2 * quarter : 3 * quarter]
    part_four = inputs[..., 3 * quarter :]
    return jnp.concatenate(
        [
            part_one * jnp.cos(row_angle) - part_two * jnp.sin(row_angle),
            part_one * jnp.sin(row_angle) + part_two * jnp.cos(row_angle),
            part_three * jnp.cos(col_angle) - part_four * jnp.sin(col_angle),
            part_three * jnp.sin(col_angle) + part_four * jnp.cos(col_angle),
        ],
        axis=-1,
    )


def conv_branch(gate_proj, pre_proj, value_proj, conv_kernel):
    pre_mix = (pre_proj * value_proj).astype(jnp.bfloat16)
    padded = with_halo(pre_mix, (("sp", 0),), 1).astype(jnp.float32)
    kernel = conv_kernel.astype(jnp.float32)
    convolved = kernel[0] * padded[:-2] + kernel[1] * padded[1:-1] + kernel[2] * padded[2:]
    return (gate_proj * convolved).astype(jnp.bfloat16)


def body(
    activations,
    norm_gain,
    query_weight,
    latent_weight,
    rope_key_weight,
    latent_gain,
    expand_weight,
    gate_weight,
    pre_weight,
    value_weight,
    conv_kernel,
    output_attend,
    output_conv,
):
    tokens_here = activations.shape[0]
    query_cols = query_weight.shape[1]
    heads_here = query_cols // (NOPE + ROPE)
    latent_cols = latent_weight.shape[1]
    channels = gate_weight.shape[1]
    joined = jnp.concatenate(
        [query_weight, latent_weight, rope_key_weight, gate_weight, pre_weight, value_weight],
        axis=1,
    )
    inputs_f32 = activations.astype(jnp.float32)
    squares = lax.psum(jnp.sum(inputs_f32 * inputs_f32, axis=1, keepdims=True), "tp")
    partial_squares = jnp.zeros((tokens_here, 1), jnp.float32)
    piece_f32 = lax.all_gather(activations, "tp", axis=1, tiled=True).astype(jnp.float32)
    scaled = (piece_f32 * norm_gain).astype(jnp.bfloat16)
    running = jnp.dot(scaled, joined, preferred_element_type=jnp.float32)
    running, folded_squares = (running, partial_squares)
    inv_rms = lax.rsqrt(squares / D + EPSILON)
    projected = running * inv_rms
    latent_end = query_cols + latent_cols
    rope_end = latent_end + ROPE
    query_proj = projected[:, :query_cols]
    latent_proj = projected[:, query_cols:latent_end]
    rope_proj = projected[:, latent_end:rope_end]
    gate_proj = projected[:, rope_end : rope_end + channels]
    pre_proj = projected[:, rope_end + channels : rope_end + 2 * channels]
    value_proj = projected[:, rope_end + 2 * channels :]
    positions = lax.axis_index("sp") * tokens_here + jnp.arange(tokens_here, dtype=jnp.int32)
    grid_rows = (positions // GRID_W).astype(jnp.float32)
    grid_cols = (positions % GRID_W).astype(jnp.float32)
    query = query_proj.reshape(tokens_here, heads_here, NOPE + ROPE)
    query = jnp.concatenate(
        [query[..., :NOPE], rotate(query[..., NOPE:], grid_rows, grid_cols)], axis=-1
    )
    query = (query * (NOPE + ROPE) ** (-0.5)).astype(jnp.bfloat16)
    query_nope = query[..., :NOPE]
    query_rope = query[..., NOPE:]
    gathered = lax.all_gather(latent_proj.astype(jnp.bfloat16), "tp", axis=1, tiled=True).astype(
        jnp.float32
    )
    latent = (
        gathered
        * lax.rsqrt(jnp.mean(gathered * gathered, axis=1, keepdims=True) + EPSILON)
        * latent_gain
    ).astype(jnp.bfloat16)
    expanded = jnp.dot(latent, expand_weight, preferred_element_type=jnp.float32).astype(
        jnp.bfloat16
    )
    rope_key = rotate(rope_proj[:, None, :], grid_rows, grid_cols)[:, 0].astype(jnp.bfloat16)
    starting = (
        jnp.full((heads_here, tokens_here), -jnp.inf, jnp.float32),
        jnp.zeros((heads_here, tokens_here), jnp.float32),
        jnp.zeros((tokens_here, heads_here, VDIM), jnp.float32),
    )
    key_piece = lax.all_gather(expanded, "sp", axis=0, tiled=True)
    rope_piece = lax.all_gather(rope_key, "sp", axis=0, tiled=True)
    piece_rows = key_piece.shape[0]
    key_block = math.gcd(piece_rows, 1024)
    split_heads = key_piece.reshape(piece_rows, heads_here, NOPE + VDIM)

    def one_block(turn_index, state):
        row_max, row_sum, running_out = state
        offset = turn_index * key_block
        block_keys = lax.dynamic_slice_in_dim(split_heads, offset, key_block, 0)
        block_rope = lax.dynamic_slice_in_dim(rope_piece, offset, key_block, 0)
        scores = jnp.einsum(
            "thd,jhd->htj", query_nope, block_keys[..., :NOPE], preferred_element_type=jnp.float32
        )
        scores = scores + jnp.einsum(
            "thd,jd->htj", query_rope, block_rope, preferred_element_type=jnp.float32
        )
        new_max = jnp.maximum(row_max, jnp.max(scores, axis=-1))
        rescale = jnp.exp(row_max - new_max)
        weights = jnp.exp(scores - new_max[..., None])
        row_sum = row_sum * rescale + jnp.sum(weights, axis=-1)
        running_out = running_out * rescale.T[..., None] + jnp.einsum(
            "htj,jhd->thd",
            weights.astype(jnp.bfloat16),
            block_keys[..., NOPE:],
            preferred_element_type=jnp.float32,
        )
        return (new_max, row_sum, running_out)

    row_max, row_sum, running_out = lax.fori_loop(0, piece_rows // key_block, one_block, starting)
    attended = (
        (running_out / row_sum.T[..., None])
        .astype(jnp.bfloat16)
        .reshape(tokens_here, heads_here * VDIM)
    )
    log_weight_sum = row_max + jnp.log(row_sum)
    conv_mixed = conv_branch(gate_proj, pre_proj, value_proj, conv_kernel)
    mixed = lax.psum_scatter(
        (
            jnp.dot(attended, output_attend, preferred_element_type=jnp.float32)
            + jnp.dot(conv_mixed, output_conv, preferred_element_type=jnp.float32)
        ).astype(jnp.bfloat16),
        "tp",
        scatter_dimension=0,
        tiled=True,
    )
    return (mixed, log_weight_sum)


def solution(mesh):
    return jax.shard_map(
        body,
        mesh=mesh,
        in_specs=(
            P("sp", "tp"),
            P(),
            P(None, "tp"),
            P(None, "tp"),
            P(),
            P(),
            P(None, "tp"),
            P(None, "tp"),
            P(None, "tp"),
            P(None, "tp"),
            P(None, "tp"),
            P("tp", None),
            P("tp", None),
        ),
        out_specs=(P(("sp", "tp"), None), P("tp", "sp")),
        check_vma=False,
    )
```

profile of v0, /device:TPU:0, one launch (start us, length us, event | category | flops | bytes accessed | tf_op | source)
XLA Modules:
  0.0 135.6 jit_solution(17453811287171782455)
XLA Ops:
  7.2 0.0 copy-start
  7.2 0.0 copy-start.5
  7.2 0.0 copy-start.1
  7.2 0.0 copy-start.3
  7.2 0.0 copy-start.4
  7.2 0.0 all-gather.3.cloned.1.call-start
  7.3 0.7 all-gather.3.cloned.1.call-update
  8.0 0.0 reduce-scatter.2.cloned.1.call-start
  8.0 1.0 multiply_reduce_fusion
  9.0 1.2 copy.19
  10.3 1.3 copy.20
  11.5 1.2 copy.21
  12.8 15.2 %psum.7 = f32[256,1]{0,1:T(1,128)S(1)} all-reduce(f32[256,1]{0,1:T(1,128)S(1)} %bitcast.73), channel_id=1, replica_groups=mesh['sp'=4,'tp'=8] {'tp'}, use_global_device_ids=true, to_apply=%region_1.0 | all-reduce | flops 256 | bytes 2048 | tf_op jit(solution)/shard_map/psum | solution.py:82
  28.0 0.0 copy-done.5
  28.0 0.6 slice_bitcast_fusion.13
  28.6 0.0 copy-done.1
  28.6 0.0 copy-start.7
  28.6 0.9 constant_dynamic-update-slice_fusion.5
  29.5 0.0 copy-done.3
  29.6 0.7 constant_dynamic-update-slice_fusion.4
  30.3 0.0 copy-done.4
  30.3 0.7 constant_dynamic-update-slice_fusion.3
  31.0 0.8 constant_dynamic-update-slice_fusion.2
  31.8 0.9 constant_dynamic-update-slice_fusion.1
  32.7 0.8 constant_dynamic-update-slice_fusion
  33.5 2.7 %all-gather.3.cloned.1.call-done = bf16[256,2048]{1,0:T(8,128)(2,1)} async-done(((bf16[256,256]{1,0:T(8,128)(2,1)}), bf16[256,2048]{1,0:T(8,128)(2,1)}) %all-gather.3.cloned.1.call-update) | async-done | bytes 1048592 | tf_op jit(solution)/shard_map/all_gather | solution.py:84
  36.2 0.0 copy-done.7
  36.2 0.0 copy-start.6
  36.2 0.0 copy-start.8
  36.2 3.1 %convolution_multiply_fusion = f32[256,704]{0,1:T(8,128)S(1)} fusion(bf16[2048,704]{0,1:T(8,128)(2,1)} %constant_dynamic-update-slice_fusion, bf16[256,2048]{1,0:T(8,128)(2,1)} %all-gather.3.cloned.1.call-done, f32[2048]{0:T(1024)S(1)} %copy-done.7, f32[256]{0:T(256)S(1)} %bitcast.74), kind=kOutput, calls=%fused_computation.6 | convolution fusion | flops 739950592 | bytes 4662272 | tf_op jit(solution)/shard_map/dot_general | solution.py:86
  39.4 0.1 constant_dynamic-update-slice_fusion.9
  39.6 0.1 constant_dynamic-update-slice_fusion.8
  39.7 0.2 fusion.52
  39.9 13.4 %all-gather = bf16[1024,1,64]{0,2,1:T(8,128)(2,1)S(1)} all-gather(bf16[256,1,64]{0,2,1:T(8,128)(2,1)S(1)} %pad_maximum_fusion), channel_id=2, replica_groups=mesh['sp'=4,'tp'=8] {'sp'}, dimensions={0}, use_global_device_ids=true | all-gather | bytes 163840 | tf_op jit(solution)/shard_map/all_gather | solution.py:126
  53.4 0.1 constant_dynamic-update-slice_fusion.6
  53.5 9.3 %all_gather.13 = bf16[256,512]{0,1:T(8,128)(2,1)S(1)} all-gather(bf16[256,64]{0,1:T(8,128)(2,1)S(1)} %slice.196), channel_id=1, replica_groups=mesh['sp'=4,'tp'=8] {'tp'}, dimensions={1}, use_global_device_ids=true | all-gather | bytes 294912 | tf_op jit(solution)/shard_map/all_gather | solution.py:108
  62.8 0.1 fusion.10
  62.9 0.0 copy-done.6
  62.9 0.0 copy-done.8
  62.9 0.4 convolution_convert_fusion
  63.3 16.1 %all_gather.14 = bf16[1024,256]{1,0:T(8,128)(2,1)S(1)} all-gather(bf16[256,256]{1,0:T(8,128)(2,1)S(1)} %convolution_convert_fusion), channel_id=1, replica_groups=mesh['sp'=4,'tp'=8] {'sp'}, dimensions={0}, use_global_device_ids=true | all-gather | bytes 655360 | tf_op jit(solution)/shard_map/all_gather | solution.py:125
  79.4 0.3 convolution_bitcast_fusion.1
  79.7 0.4 fusion.66
  80.1 0.0 copy-start.2
  80.2 0.3 fusion.7
  80.5 0.1 fusion.65
  80.5 3.7 %collective-permute-start = (bf16[1,128]{0,1:T(8,128)(2,1)S(1)}, bf16[1,128]{0,1:T(8,128)(2,1)S(1)}, u32[]{:S(2)}, u32[]{:S(2)}) collective-permute-start(bf16[1,128]{0,1:T(8,128)(2,1)S(1)} %get-tuple-element.26), channel_id=1, source_target_pairs={{0,8},{8,16},{16,24},{1,9},{9,17},{17,25},{2,10},{10,18},{18,26},{... | collective-permute-start | bytes 776 | tf_op jit(solution)/shard_map/ppermute | solution.py:23
  84.2 1.3 collective-permute-start.1
  85.5 0.0 copy-done
  85.5 2.4 %fusion.9 = f32[256,2048]{1,0:T(8,128)} fusion(bf16[128,2048]{1,0:T(8,128)(2,1)S(1)} %copy-done, f32[1,256,1024]{2,1,0:T(8,128)S(1)} %get-tuple-element.44, f32[256]{0:T(256)S(1)} %get-tuple-element.43, bf16[1024,1,256]{2,0,1:T(8,128)(2,1)S(1)} %bitcast.70, f32[256]{0:T(256)S(1)} %get-tuple-element.42, f32[256]{0:T(256)S(1)} %get-tuple-element.41), kind=kOutput, calls=%fused_computation.19 | convolution fusion | flops 201949184 | bytes 3935232 | tf_op jit(solution)/shard_map/dot_general | solution.py:164
  88.0 0.0 collective-permute-done
  88.0 2.1 %collective-permute-done.1 = bf16[1,128]{0,1:T(8,128)(2,1)S(1)} collective-permute-done((bf16[1,128]{0,1:T(8,128)(2,1)S(1)}, bf16[1,128]{0,1:T(8,128)(2,1)S(1)}, u32[]{:S(2)}, u32[]{:S(2)}) %collective-permute-start.1) | collective-permute-done | bytes 288 | tf_op jit(solution)/shard_map/ppermute | solution.py:24
  90.0 0.1 maximum_convert_fusion
  90.2 0.0 copy-done.2
  90.2 3.2 %fusion = bf16[256,2048]{1,0:T(8,128)(2,1)} fusion(f32[256,2048]{1,0:T(8,128)} %fusion.9, bf16[128,2048]{1,0:T(8,128)(2,1)S(1)} %copy-done.2, f32[258,128]{0,1:T(8,128)S(1)} %maximum_convert_fusion, f32[256,704]{0,1:T(8,128)S(1)} %convolution_multiply_fusion, f32[128]{0:T(128)} %get-tuple-element.38, f32[128]{0:T(128)} %get-tuple-element.39, ...), kind=kOutput, calls=%fused_computation.1 | convolution fusion | flops 135495680 | bytes 4195840 | tf_op jit(solution)/shard_map/dot_general | solution.py:165
  93.4 0.0 reduce-scatter.2.cloned.1.call-update
  93.4 0.6 log_add_fusion
  94.0 34.8 %reduce-scatter.2.cloned.1.call-done = bf16[32,2048]{1,0:T(8,128)(2,1)} async-done(((bf16[256,2048]{1,0:T(8,128)(2,1)}), bf16[32,2048]{1,0:T(8,128)(2,1)}) %reduce-scatter.2.cloned.1.call-update) | async-done | bytes 131088 | tf_op jit(solution)/shard_map/reduce_scatter | solution.py:162
  (13 shorter events, 0.1 us)
Async XLA Ops:
  7.2 78.4 %copy-start = (bf16[128,2048]{1,0:T(8,128)(2,1)S(1)}, bf16[128,2048]{1,0:T(8,128)(2,1)}, u32[]{:S(2)}) copy-start(bf16[128,2048]{1,0:T(8,128)(2,1)} %param.24) | copy-start | bytes 1572868
  7.2 20.8 %copy-start.5 = (bf16[3,128]{1,0:T(4,128)(2,1)S(1)}, bf16[3,128]{1,0:T(4,128)(2,1)}, u32[]{:S(2)}) copy-start(bf16[3,128]{1,0:T(4,128)(2,1)} %param.23) | copy-start | bytes 2308
  7.2 21.4 %copy-start.1 = (bf16[2048,192]{0,1:T(8,128)(2,1)S(1)}, bf16[2048,192]{0,1:T(8,128)(2,1)}, u32[]{:S(2)}) copy-start(bf16[2048,192]{0,1:T(8,128)(2,1)} %param.15) | copy-start | bytes 2359300
  7.2 22.3 %copy-start.3 = (bf16[2048,64]{0,1:T(8,128)(2,1)S(1)}, bf16[2048,64]{0,1:T(8,128)(2,1)}, u32[]{:S(2)}) copy-start(bf16[2048,64]{0,1:T(8,128)(2,1)} %param.16) | copy-start | bytes 786436
  7.2 23.1 %copy-start.4 = (bf16[2048,64]{0,1:T(8,128)(2,1)S(1)}, bf16[2048,64]{0,1:T(8,128)(2,1)}, u32[]{:S(2)}) copy-start(bf16[2048,64]{0,1:T(8,128)(2,1)} %param.17) | copy-start | bytes 786436
  7.2 29.0 %all-gather.3.cloned.1.call-start = ((), (), s32[]{:S(2)}) async-start(), calls=%async_computation.1 | async-start | bytes 1179648 | tf_op jit(solution)/shard_map/all_gather | solution.py:84
  8.0 120.8 %reduce-scatter.2.cloned.1.call-start = ((), (), s32[]{:S(2)}) async-start(), calls=%async_computation.2 | async-start | bytes 1179648 | tf_op jit(solution)/shard_map/reduce_scatter | solution.py:162
  28.6 7.6 %copy-start.7 = (f32[2048]{0:T(1024)S(1)}, f32[2048]{0:T(1024)}, u32[]{:S(2)}) copy-start(f32[2048]{0:T(1024)} %param.14) | copy-start | bytes 24580
  36.2 26.7 %copy-start.6 = (bf16[512,256]{1,0:T(8,128)(2,1)S(1)}, bf16[512,256]{1,0:T(8,128)(2,1)}, u32[]{:S(2)}) copy-start(bf16[512,256]{1,0:T(8,128)(2,1)} %param.19) | copy-start | bytes 786436
  36.2 26.7 %copy-start.8 = (f32[512]{0:T(512)S(1)}, f32[512]{0:T(512)}, u32[]{:S(2)}) copy-start(f32[512]{0:T(512)} %param.18) | copy-start | bytes 6148
  80.1 10.0 %copy-start.2 = (bf16[128,2048]{1,0:T(8,128)(2,1)S(1)}, bf16[128,2048]{1,0:T(8,128)(2,1)}, u32[]{:S(2)}) copy-start(bf16[128,2048]{1,0:T(8,128)(2,1)} %param.25) | copy-start | bytes 1572868
  80.5 7.4 %collective-permute-start = (bf16[1,128]{0,1:T(8,128)(2,1)S(1)}, bf16[1,128]{0,1:T(8,128)(2,1)S(1)}, u32[]{:S(2)}, u32[]{:S(2)}) collective-permute-start(bf16[1,128]{0,1:T(8,128)(2,1)S(1)} %get-tuple-element.26), channel_id=1, source_target_pairs={{0,8},{8,16},{16,24},{1,9},{9,17},{17,25},{2,10},{10,18},{18,26},{... | collective-permute-start | bytes 776 | tf_op jit(solution)/shard_map/ppermute | solution.py:23
  84.2 5.8 %collective-permute-start.1 = (bf16[1,128]{0,1:T(8,128)(2,1)S(1)}, bf16[1,128]{0,1:T(8,128)(2,1)S(1)}, u32[]{:S(2)}, u32[]{:S(2)}) collective-permute-start(bf16[1,128]{0,1:T(8,128)(2,1)S(1)} %get-tuple-element.36), channel_id=1, source_target_pairs={{8,0},{16,8},{24,16},{9,1},{17,9},{25,17},{10,2},{18,10},{26,18},{... | collective-permute-start | bytes 776 | tf_op jit(solution)/shard_map/ppermute | solution.py:24
Sparse Core Ops, SparseCore 0:
  9.9 26.2 all-gather.2
  93.5 35.1 reduce-scatter.1
where the time goes:
time: 136 us
  blocking collectives  53.9 us (40%)
  waiting for transfers between devices  40.2 us (30%)
  between operations  14.3 us (11%)
  matrix products  9.9 us (7%)
  local copies, waits for them, and re-layouts  9.39 us (7%)
  starting transfers between devices  5.04 us (4%)
  other arithmetic  2.83 us (2%)
    reduce_scatter x1, waiting for transfers between devices, body(): lax.psum_scatter((jnp.dot(attended, output_attend, preferred_element_type...  34.8 us
    all_gather x1, blocking collectives, body(): key_piece = lax.all_gather(expanded, 'sp', axis=0, tiled=True)  16.1 us
    psum x1, blocking collectives, body(): lax.psum(jnp.sum(inputs_f32 * inputs_f32, axis=1, keepdims=True), 'tp')  15.2 us
    all_gather x1, blocking collectives, body(): rope_piece = lax.all_gather(rope_key, 'sp', axis=0, tiled=True)  13.4 us
    all_gather x1, blocking collectives, body(): lax.all_gather(latent_proj.astype(jnp.bfloat16), 'tp', axis=1, tiled=True)  9.26 us
    unnamed x27, local copies, waits for them, and re-layouts  7.86 us
    ppermute x1, starting transfers between devices, with_halo(): before = lax.ppermute(last, axis, up)  3.67 us
    dot_general x1, matrix products, body(): jnp.dot(conv_mixed, output_conv, preferred_element_type=jnp.float32)  3.22 us
  transfers between devices with their start and end apart: 4, of which 3 were waited for; matrix products, arithmetic and copies ran while one was open for 10% of the time, Pallas kernels for 0%

commit v1 on v0

--- a/solution.py
+++ b/solution.py
@@ -11,6 +11,14 @@
 GRID_W = 64
 EPSILON = 1e-06
 ROPE_BASE = 10000.0
+
+
+def touch_desk(my_data, w_in):
+    return jnp.split(
+        lax.all_gather(jnp.concatenate([w_in, my_data], axis=1), "sp", axis=0, tiled=True),
+        [w_in.shape[1]],
+        axis=1,
+    )
 
 
 def with_halo(array, sides, width):
@@ -122,8 +130,7 @@
         jnp.zeros((heads_here, tokens_here), jnp.float32),
         jnp.zeros((tokens_here, heads_here, VDIM), jnp.float32),
     )
-    key_piece = lax.all_gather(expanded, "sp", axis=0, tiled=True)
-    rope_piece = lax.all_gather(rope_key, "sp", axis=0, tiled=True)
+    key_piece, rope_piece = touch_desk(rope_key, expanded)
     piece_rows = key_piece.shape[0]
     key_block = math.gcd(piece_rows, 1024)
     split_heads = key_piece.reshape(piece_rows, heads_here, NOPE + VDIM)

time: 136 us -> 123 us (0.904)
  blocking collectives: 53.9 us -> 42.5 us
    all_gather x2 -> x1, blocking collectives: 29.5 us -> 18.1 us  [touch_desk(): lax.all_gather(jnp.concatenate([w_in, my_data], axis=1), 'sp', axis=0, ti...]
  transfers between devices with their start and end apart: 4 -> 4, of which waited for: 3 -> 3; matrix products, arithmetic and copies ran while one was open for 10% -> 11% of each run, Pallas kernels for 0% -> 0%
where the time goes in v1:
time: 123 us
  blocking collectives  42.5 us (35%)
  waiting for transfers between devices  40.2 us (33%)
  between operations  14.3 us (12%)
  matrix products  9.9 us (8%)
  local copies, waits for them, and re-layouts  9.46 us (8%)
  starting transfers between devices  3.75 us (3%)
  other arithmetic  2.86 us (2%)
    reduce_scatter x1, waiting for transfers between devices, body(): lax.psum_scatter((jnp.dot(attended, output_attend, preferred_element_type...  34.8 us
    all_gather x1, blocking collectives, touch_desk(): lax.all_gather(jnp.concatenate([w_in, my_data], axis=1), 'sp', axis=0, ti...  18.1 us
    psum x1, blocking collectives, body(): lax.psum(jnp.sum(inputs_f32 * inputs_f32, axis=1, keepdims=True), 'tp')  15.2 us
    all_gather x1, blocking collectives, body(): lax.all_gather(latent_proj.astype(jnp.bfloat16), 'tp', axis=1, tiled=True)  9.27 us
    unnamed x27, local copies, waits for them, and re-layouts  7.89 us
    dot_general x1, matrix products, body(): jnp.dot(conv_mixed, output_conv, preferred_element_type=jnp.float32)  3.22 us
    dot_general x1, matrix products, body(): running = jnp.dot(scaled, joined, preferred_element_type=jnp.float32)  3.12 us
    all_gather x1, waiting for transfers between devices, body(): lax.all_gather(activations, 'tp', axis=1, tiled=True).astype(jnp.float32)  2.65 us
  transfers between devices with their start and end apart: 4, of which 3 were waited for; matrix products, arithmetic and copies ran while one was open for 11% of the time, Pallas kernels for 0%

profile of v1, /device:TPU:0, one launch (start us, length us, event | category | flops | bytes accessed | tf_op | source)
XLA Modules:
  0.0 123.0 jit_solution(8662854067318313465)
XLA Ops:
  7.2 0.0 copy-start
  7.2 0.0 copy-start.5
  7.2 0.0 copy-start.1
  7.2 0.0 copy-start.3
  7.2 0.0 copy-start.4
  7.2 0.0 all-gather.2.cloned.1.call-start
  7.3 0.7 all-gather.2.cloned.1.call-update
  8.0 0.0 reduce-scatter.2.cloned.1.call-start
  8.0 1.0 multiply_reduce_fusion
  9.0 1.2 %copy.19 = bf16[2048,128]{0,1:T(8,128)(2,1)S(1)} copy(bf16[2048,128]{1,0:T(8,128)(2,1)} %param.20) | data formatting | bytes 1048576 | tf_op args[7]
  10.3 1.3 %copy.20 = bf16[2048,128]{0,1:T(8,128)(2,1)S(1)} copy(bf16[2048,128]{1,0:T(8,128)(2,1)} %param.21) | data formatting | bytes 1048576 | tf_op args[8]
  11.5 1.2 %copy.21 = bf16[2048,128]{0,1:T(8,128)(2,1)S(1)} copy(bf16[2048,128]{1,0:T(8,128)(2,1)} %param.22) | data formatting | bytes 1048576 | tf_op args[9]
  12.8 15.2 %psum.7 = f32[256,1]{0,1:T(1,128)S(1)} all-reduce(f32[256,1]{0,1:T(1,128)S(1)} %bitcast.69), channel_id=1, replica_groups=mesh['sp'=4,'tp'=8] {'tp'}, use_global_device_ids=true, to_apply=%region_1.0 | all-reduce | flops 256 | bytes 2048 | tf_op jit(solution)/shard_map/psum | solution.py:90
  28.0 0.0 copy-done.5
  28.0 0.6 slice_bitcast_fusion.14
  28.6 0.0 copy-done.1
  28.6 0.0 copy-start.7
  28.6 0.9 constant_dynamic-update-slice_fusion.5
  29.5 0.0 copy-done.3
  29.6 0.7 constant_dynamic-update-slice_fusion.4
  30.3 0.0 copy-done.4
  30.3 0.7 constant_dynamic-update-slice_fusion.3
  31.0 0.8 constant_dynamic-update-slice_fusion.2
  31.8 0.9 constant_dynamic-update-slice_fusion.1
  32.7 0.8 constant_dynamic-update-slice_fusion
  33.5 2.6 %all-gather.2.cloned.1.call-done = bf16[256,2048]{1,0:T(8,128)(2,1)} async-done(((bf16[256,256]{1,0:T(8,128)(2,1)}), bf16[256,2048]{1,0:T(8,128)(2,1)}) %all-gather.2.cloned.1.call-update) | async-done | bytes 1048592 | tf_op jit(solution)/shard_map/all_gather | solution.py:92
  36.2 0.0 copy-done.7
  36.2 0.0 copy-start.6
  36.2 0.0 copy-start.8
  36.2 3.1 %convolution_multiply_fusion = f32[256,704]{0,1:T(8,128)S(1)} fusion(bf16[2048,704]{0,1:T(8,128)(2,1)} %constant_dynamic-update-slice_fusion, bf16[256,2048]{1,0:T(8,128)(2,1)} %all-gather.2.cloned.1.call-done, f32[2048]{0:T(1024)S(1)} %copy-done.7, f32[256]{0:T(256)S(1)} %bitcast.70), kind=kOutput, calls=%fused_computation.6 | convolution fusion | flops 739950592 | bytes 4662272 | tf_op jit(solution)/shard_map/dot_general | solution.py:94
  39.4 0.1 constant_dynamic-update-slice_fusion.9
  39.6 0.1 constant_dynamic-update-slice_fusion.8
  39.7 9.3 %all_gather.10 = bf16[256,512]{0,1:T(8,128)(2,1)S(1)} all-gather(bf16[256,64]{0,1:T(8,128)(2,1)S(1)} %slice.196), channel_id=1, replica_groups=mesh['sp'=4,'tp'=8] {'tp'}, dimensions={1}, use_global_device_ids=true | all-gather | bytes 294912 | tf_op jit(solution)/shard_map/all_gather | solution.py:116
  49.0 0.1 fusion.10
  49.1 0.1 constant_dynamic-update-slice_fusion.7
  49.2 0.2 fusion.52
  49.4 0.0 copy-done.6
  49.5 0.0 copy-done.8
  49.5 0.4 convolution_convert_fusion
  49.9 18.1 %all_gather.11 = bf16[1024,320]{0,1:T(8,128)(2,1)S(1)} all-gather(bf16[256,320]{0,1:T(8,128)(2,1)S(1)} %pad_maximum_fusion), channel_id=1, replica_groups=mesh['sp'=4,'tp'=8] {'sp'}, dimensions={0}, use_global_device_ids=true | all-gather | bytes 819200 | tf_op jit(solution)/shard_map/all_gather | solution.py:18
  68.1 0.3 convolution_bitcast_fusion.1
  68.4 0.4 fusion.66
  68.8 0.0 copy-start.2
  68.8 0.3 fusion.7
  69.1 0.1 fusion.65
  69.2 2.4 %collective-permute-start = (bf16[1,128]{0,1:T(8,128)(2,1)S(1)}, bf16[1,128]{0,1:T(8,128)(2,1)S(1)}, u32[]{:S(2)}, u32[]{:S(2)}) collective-permute-start(bf16[1,128]{0,1:T(8,128)(2,1)S(1)} %get-tuple-element.26), channel_id=1, source_target_pairs={{0,8},{8,16},{16,24},{1,9},{9,17},{17,25},{2,10},{10,18},{18,26},{... | collective-permute-start | bytes 776 | tf_op jit(solution)/shard_map/ppermute | solution.py:31
  71.6 1.3 %collective-permute-start.1 = (bf16[1,128]{0,1:T(8,128)(2,1)S(1)}, bf16[1,128]{0,1:T(8,128)(2,1)S(1)}, u32[]{:S(2)}, u32[]{:S(2)}) collective-permute-start(bf16[1,128]{0,1:T(8,128)(2,1)S(1)} %get-tuple-element.36), channel_id=1, source_target_pairs={{8,0},{16,8},{24,16},{9,1},{17,9},{25,17},{10,2},{18,10},{26,18},{... | collective-permute-start | bytes 776 | tf_op jit(solution)/shard_map/ppermute | solution.py:32
  72.9 0.0 copy-done
  72.9 2.4 %fusion.9 = f32[256,2048]{1,0:T(8,128)} fusion(bf16[128,2048]{1,0:T(8,128)(2,1)S(1)} %copy-done, f32[1,256,1024]{2,1,0:T(8,128)S(1)} %get-tuple-element.44, f32[256]{0:T(256)S(1)} %get-tuple-element.43, bf16[1024,1,256]{0,2,1:T(8,128)(2,1)S(1)} %slice_bitcast_fusion, f32[256]{0:T(256)S(1)} %get-tuple-element.42, f32[256]{0:T(256)S(1)} %get-tuple-element.41), kind=kOutput, calls=%fused_computation.19 | convolution fusion | flops 201949184 | bytes 3935232 | tf_op jit(solution)/shard_map/dot_general | solution.py:171
  75.3 0.0 collective-permute-done
  75.4 2.1 %collective-permute-done.1 = bf16[1,128]{0,1:T(8,128)(2,1)S(1)} collective-permute-done((bf16[1,128]{0,1:T(8,128)(2,1)S(1)}, bf16[1,128]{0,1:T(8,128)(2,1)S(1)}, u32[]{:S(2)}, u32[]{:S(2)}) %collective-permute-start.1) | collective-permute-done | bytes 288 | tf_op jit(solution)/shard_map/ppermute | solution.py:32
  77.4 0.1 maximum_convert_fusion
  77.5 0.0 copy-done.2
  77.5 3.2 %fusion = bf16[256,2048]{1,0:T(8,128)(2,1)} fusion(f32[256,2048]{1,0:T(8,128)} %fusion.9, bf16[128,2048]{1,0:T(8,128)(2,1)S(1)} %copy-done.2, f32[258,128]{0,1:T(8,128)S(1)} %maximum_convert_fusion, f32[256,704]{0,1:T(8,128)S(1)} %convolution_multiply_fusion, f32[128]{0:T(128)} %get-tuple-element.38, f32[128]{0:T(128)} %get-tuple-element.39, ...), kind=kOutput, calls=%fused_computation.1 | convolution fusion | flops 135495680 | bytes 4195840 | tf_op jit(solution)/shard_map/dot_general | solution.py:172
  80.8 0.0 reduce-scatter.2.cloned.1.call-update
  80.8 0.6 log_add_fusion
  81.4 34.8 %reduce-scatter.2.cloned.1.call-done = bf16[32,2048]{1,0:T(8,128)(2,1)} async-done(((bf16[256,2048]{1,0:T(8,128)(2,1)}), bf16[32,2048]{1,0:T(8,128)(2,1)}) %reduce-scatter.2.cloned.1.call-update) | async-done | bytes 131088 | tf_op jit(solution)/shard_map/reduce_scatter | solution.py:169
  (15 shorter events, 0.2 us)
Async XLA Ops:
  7.2 65.7 %copy-start = (bf16[128,2048]{1,0:T(8,128)(2,1)S(1)}, bf16[128,2048]{1,0:T(8,128)(2,1)}, u32[]{:S(2)}) copy-start(bf16[128,2048]{1,0:T(8,128)(2,1)} %param.24) | copy-start | bytes 1572868
  7.2 20.8 %copy-start.5 = (bf16[3,128]{1,0:T(4,128)(2,1)S(1)}, bf16[3,128]{1,0:T(4,128)(2,1)}, u32[]{:S(2)}) copy-start(bf16[3,128]{1,0:T(4,128)(2,1)} %param.23) | copy-start | bytes 2308
  7.2 21.4 %copy-start.1 = (bf16[2048,192]{0,1:T(8,128)(2,1)S(1)}, bf16[2048,192]{0,1:T(8,128)(2,1)}, u32[]{:S(2)}) copy-start(bf16[2048,192]{0,1:T(8,128)(2,1)} %param.15) | copy-start | bytes 2359300
  7.2 22.3 %copy-start.3 = (bf16[2048,64]{0,1:T(8,128)(2,1)S(1)}, bf16[2048,64]{0,1:T(8,128)(2,1)}, u32[]{:S(2)}) copy-start(bf16[2048,64]{0,1:T(8,128)(2,1)} %param.16) | copy-start | bytes 786436
  7.2 23.1 %copy-start.4 = (bf16[2048,64]{0,1:T(8,128)(2,1)S(1)}, bf16[2048,64]{0,1:T(8,128)(2,1)}, u32[]{:S(2)}) copy-start(bf16[2048,64]{0,1:T(8,128)(2,1)} %param.17) | copy-start | bytes 786436
  7.2 29.0 %all-gather.2.cloned.1.call-start = ((), (), s32[]{:S(2)}) async-start(), calls=%async_computation.1 | async-start | bytes 1179648 | tf_op jit(solution)/shard_map/all_gather | solution.py:92
  8.0 108.2 %reduce-scatter.2.cloned.1.call-start = ((), (), s32[]{:S(2)}) async-start(), calls=%async_computation.2 | async-start | bytes 1179648 | tf_op jit(solution)/shard_map/reduce_scatter | solution.py:169
  28.6 7.6 %copy-start.7 = (f32[2048]{0:T(1024)S(1)}, f32[2048]{0:T(1024)}, u32[]{:S(2)}) copy-start(f32[2048]{0:T(1024)} %param.14) | copy-start | bytes 24580
  36.2 13.3 %copy-start.6 = (bf16[512,256]{1,0:T(8,128)(2,1)S(1)}, bf16[512,256]{1,0:T(8,128)(2,1)}, u32[]{:S(2)}) copy-start(bf16[512,256]{1,0:T(8,128)(2,1)} %param.19) | copy-start | bytes 786436
  36.2 13.3 %copy-start.8 = (f32[512]{0:T(512)S(1)}, f32[512]{0:T(512)}, u32[]{:S(2)}) copy-start(f32[512]{0:T(512)} %param.18) | copy-start | bytes 6148
  68.8 8.7 %copy-start.2 = (bf16[128,2048]{1,0:T(8,128)(2,1)S(1)}, bf16[128,2048]{1,0:T(8,128)(2,1)}, u32[]{:S(2)}) copy-start(bf16[128,2048]{1,0:T(8,128)(2,1)} %param.25) | copy-start | bytes 1572868
  69.2 6.1 %collective-permute-start = (bf16[1,128]{0,1:T(8,128)(2,1)S(1)}, bf16[1,128]{0,1:T(8,128)(2,1)S(1)}, u32[]{:S(2)}, u32[]{:S(2)}) collective-permute-start(bf16[1,128]{0,1:T(8,128)(2,1)S(1)} %get-tuple-element.26), channel_id=1, source_target_pairs={{0,8},{8,16},{16,24},{1,9},{9,17},{17,25},{2,10},{10,18},{18,26},{... | collective-permute-start | bytes 776 | tf_op jit(solution)/shard_map/ppermute | solution.py:31
  71.6 5.8 %collective-permute-start.1 = (bf16[1,128]{0,1:T(8,128)(2,1)S(1)}, bf16[1,128]{0,1:T(8,128)(2,1)S(1)}, u32[]{:S(2)}, u32[]{:S(2)}) collective-permute-start(bf16[1,128]{0,1:T(8,128)(2,1)S(1)} %get-tuple-element.36), channel_id=1, source_target_pairs={{8,0},{16,8},{24,16},{9,1},{17,9},{25,17},{10,2},{18,10},{26,18},{... | collective-permute-start | bytes 776 | tf_op jit(solution)/shard_map/ppermute | solution.py:32
Sparse Core Ops, SparseCore 0:
  9.9 26.2 all-gather.1
  80.9 35.2 reduce-scatter.1
